TPU v7x, 512 devices: a whole 4x4x16 slice. The times are simulated.
512 devices in a mesh: kv: 32 (over z, core), tp: 16 (over y, x).
Axes of the slice: x: 4, y: 4, z: 16, core: 2. Of those that a mesh axis runs over, the one named last changes fastest.
Arguments:
- tokens: bfloat16 [16, 2048], P(None, 'kv'), may hold values from -8 to 8
- lengths: int32 [16], replicated, may hold values from 1 to 49152, 196608 in all
- latent_cache: bfloat16 [16, 49152, 256], P(None, ('kv', 'tp')), may hold values from -10 to 10
- rope_cache: bfloat16 [16, 49152, 32], P(None, ('kv', 'tp')), may hold values from -2000 to 2000
- gain_in: bfloat16 [2048], P('kv'), may hold values from 0.099609375 to 1.8984375
- w_down_q: bfloat16 [2048, 512], P('kv'), may hold values from -0.125 to 0.125
- w_down_kv: bfloat16 [2048, 256], P('kv'), may hold values from -0.125 to 0.125
- w_rope_key: bfloat16 [2048, 32], P('kv'), may hold values from -0.125 to 0.125
- gain_q: bfloat16 [512], replicated, may hold values from 0.099609375 to 1.8984375
- w_up_qn: bfloat16 [512, 16, 64], replicated, may hold values from -0.25 to 0.25
- w_up_qr: bfloat16 [512, 16, 32], replicated, may hold values from -0.25 to 0.25
- gain_kv: bfloat16 [256], replicated, may hold values from 0.099609375 to 1.8984375
- w_key_up: bfloat16 [256, 16, 64], replicated, may hold values from -0.375 to 0.375
- w_value_up: bfloat16 [256, 16, 64], replicated, may hold values from -0.375 to 0.375
- w_attn_out: bfloat16 [16, 64, 2048], P('tp', None, 'kv'), may hold values from -0.1875 to 0.1875
- gain_mid: bfloat16 [2048], P('kv'), may hold values from 0.099609375 to 1.8984375
- w_ff_in: bfloat16 [2048, 8192], P('kv', 'tp'), may hold values from -0.125 to 0.125
- w_ff_out: bfloat16 [8192, 2048], P('tp', 'kv'), may hold values from -0.0625 to 0.0625
Outputs:
- mixed: bfloat16 [16, 2048], P(None, 'kv')
- new_latent: bfloat16 [16, 256], replicated
- new_rope_key: bfloat16 [16, 32], replicated
Inputs may be any that keep to these rules, and one draw needn't show every extreme that they name: `lengths`: each sequence's live cache positions; one sequence fills the whole cache.
All inputs are finite; a program needn't handle non-finite values.
Results may differ from a plain program's by a relative error of at most 0.012.
Values sent between devices are 32-bit elements; how exact they have to be, the bound alone decides.
A program may use at most 64 MiB of HBM per device.

v0:
```python
import jax
import jax.numpy as jnp
from jax import lax
from jax.sharding import Mesh
from jax.sharding import PartitionSpec as P

D = 2048
NOPE = 64
ROPE = 32
KV = ("kv_0", "kv_1")
KV_TP = ("kv_0", "kv_1", "tp_0", "tp_1")
TP = ("tp_0", "tp_1")
EPS = 1e-06


def over_axes(value, axes):
    for axis in axes:
        value = lax.psum(value, axis)
    return value


def copy_for_each(value, axis):
    size = lax.axis_size(axis)
    return lax.all_to_all(
        jnp.broadcast_to(value[None], (size, *value.shape)), axis, 0, 0, tiled=True
    )


def gathered_once(value, axis):
    leaves = jax.tree.leaves(value)
    order = sorted(range(len(leaves)), key=lambda k: -leaves[k].size)
    width = (1, *leaves[order[0]].shape)[-1]
    lines = [
        jnp.pad(leaves[k].reshape(-1), (0, -leaves[k].size % width)).reshape(-1, width)
        for k in order
    ]
    both, at, found = (copy_for_each(jnp.concatenate(lines), axis), 0, {})
    for k, line in zip(order, lines):
        piece = both[:, at : at + len(line)].reshape(len(both), -1)
        found[k] = piece[:, : leaves[k].size].reshape(-1, *leaves[k].shape)
        at += len(line)
    numbers = iter(range(len(leaves)))
    return jax.tree.map(lambda _: found[next(numbers)], value)


def joined_by_halves(pieces, combine):
    while len(jax.tree.leaves(pieces)[0]) > 1:
        pieces = jax.vmap(combine)(
            *(jax.tree.map(lambda part: part[side::2], pieces) for side in (0, 1))
        )
    return jax.tree.map(lambda part: part[0], pieces)


def joined_all(value, axis, combine):
    pieces = gathered_once(value, axis)
    return joined_by_halves(pieces, combine)


def of_everyone(value, axis):
    everything = copy_for_each(value, axis)
    return jnp.sum(everything, axis=0)


def in_one(arrays, axis):
    ravelled, at, outs = (jnp.concatenate([a.reshape(-1) for a in arrays]), 0, [])
    subtotal = of_everyone(ravelled, axis)
    for a in arrays:
        outs.append(subtotal[at : at + a.size].reshape(a.shape))
        at += a.size
    return tuple(outs)


def rotate(values, positions):
    half = values.shape[-1] // 2
    inverse = 10000.0 ** (-jnp.arange(half, dtype=jnp.float32) / half)
    angle = positions.astype(jnp.float32)[:, None, None] * inverse[None, None, :]
    first = values[..., :half]
    second = values[..., half:]
    return jnp.concatenate(
        [
            first * jnp.cos(angle) - second * jnp.sin(angle),
            second * jnp.cos(angle) + first * jnp.sin(angle),
        ],
        axis=-1,
    )


def rms_scaled(values, gain):
    return (
        values
        * lax.rsqrt(jnp.mean(values * values, axis=-1, keepdims=True) + EPS)
        * gain.astype(jnp.float32)
    )


def combine(earlier, later):
    top_a, total_a, acc_a = earlier
    top_b, total_b, acc_b = later
    top = jnp.maximum(top_a, top_b)
    fade_a = jnp.exp(top_a - top)
    fade_b = jnp.exp(top_b - top)
    return (
        top,
        total_a * fade_a + total_b * fade_b,
        acc_a * fade_a[..., None] + acc_b * fade_b[..., None],
    )


def fold_sources(parts):
    tops, totals, accs = parts
    top = jnp.max(tops, axis=0)
    fade = jnp.exp(tops - top[None])
    return (top, jnp.sum(totals * fade, axis=0), jnp.sum(accs * fade[..., None], axis=0))


def per_device(
    tokens,
    lengths,
    latent_cache,
    rope_cache,
    gain_in,
    w_down_q,
    w_down_kv,
    w_rope_key,
    gain_q,
    w_up_qn,
    w_up_qr,
    gain_kv,
    w_key_up,
    w_value_up,
    w_attn_out,
    gain_mid,
    w_ff_in,
    w_ff_out,
):
    f32 = jnp.float32
    bf16 = jnp.bfloat16
    scale = (NOPE + ROPE) ** (-0.5)
    resid = tokens.astype(f32)
    scaled_in = (resid * gain_in.astype(f32)).astype(bf16)
    part_q = jnp.dot(scaled_in, w_down_q, preferred_element_type=f32)
    part_kv = jnp.dot(scaled_in, w_down_kv, preferred_element_type=f32)
    part_rope = jnp.dot(scaled_in, w_rope_key, preferred_element_type=f32)
    square_in = jnp.sum(resid * resid, axis=1)
    sum_q, sum_kv, sum_rope, total_in = (
        over_axes(part_q, KV),
        over_axes(part_kv, KV),
        over_axes(part_rope, KV),
        over_axes(square_in, KV),
    )
    inv_in = lax.rsqrt(total_in / D + EPS)[:, None]
    query_latent = rms_scaled(inv_in * sum_q, gain_q).astype(bf16)
    new_latent = rms_scaled(inv_in * sum_kv, gain_kv).astype(bf16)
    new_rope_key = rotate((inv_in * sum_rope)[:, None, :], lengths)[:, 0, :].astype(bf16)
    query_nope = jnp.einsum(
        "bc,chd->bhd", query_latent, w_up_qn, preferred_element_type=f32
    ).astype(bf16)
    query_rope = rotate(
        jnp.einsum("bc,chr->bhr", query_latent, w_up_qr, preferred_element_type=f32), lengths
    ).astype(bf16)
    query_cache = jnp.einsum(
        "bhd,khd->bhk", query_nope, w_key_up, preferred_element_type=f32
    ).astype(bf16)
    rows = latent_cache.shape[1]
    positions = lax.axis_index(KV_TP) * rows + jnp.arange(rows, dtype=jnp.int32)
    live = (positions[None, :] < lengths[:, None])[:, None, :]
    scores = (
        jnp.einsum("bhk,blk->bhl", query_cache, latent_cache, preferred_element_type=f32)
        + jnp.einsum("bhr,blr->bhl", query_rope, rope_cache, preferred_element_type=f32)
    ) * scale
    scores = jnp.where(live, scores, -1e30)
    top = jnp.max(scores, axis=2)
    weights = jnp.where(live, jnp.exp(scores - top[:, :, None]), 0.0)
    total = jnp.sum(weights, axis=2)
    acc = jnp.einsum("bhl,blk->bhk", weights.astype(bf16), latent_cache, preferred_element_type=f32)
    heads_dev = w_attn_out.shape[0]
    first_head = lax.axis_index(TP) * heads_dev
    own_value_up = lax.dynamic_slice_in_dim(w_value_up, first_head, heads_dev, 1).astype(f32)
    own_cache_q = lax.dynamic_slice_in_dim(query_cache, first_head, heads_dev, 1)
    own_rope_q = lax.dynamic_slice_in_dim(query_rope, first_head, heads_dev, 1)
    self_score = (
        jnp.einsum("bhk,bk->bh", own_cache_q, new_latent, preferred_element_type=f32)
        + jnp.einsum("bhr,br->bh", own_rope_q, new_rope_key, preferred_element_type=f32)
    ) * scale
    expanded = jnp.einsum("bhk,khv->bhv", acc, w_value_up.astype(f32))
    top, total, expanded = fold_sources(
        (
            lax.all_to_all(top[None], TP, split_axis=2, concat_axis=0, tiled=True),
            lax.all_to_all(total[None], TP, split_axis=2, concat_axis=0, tiled=True),
            lax.all_to_all(expanded[None], TP, split_axis=2, concat_axis=0, tiled=True),
        )
    )
    top, total, expanded = joined_all((top, total, expanded), KV, combine)
    joined = jnp.maximum(top, self_score)
    fade = jnp.exp(top - joined)
    self_weight = jnp.exp(self_score - joined)
    total = total * fade + self_weight
    self_value = jnp.einsum("bk,khv->bhv", new_latent.astype(f32), own_value_up)
    expanded = (
        expanded * fade[:, :, None] + self_weight.astype(bf16).astype(f32)[:, :, None] * self_value
    )
    head_out = (expanded / total[:, :, None]).astype(bf16)
    attn_part = jnp.einsum("bhv,hvd->bd", head_out, w_attn_out, preferred_element_type=f32)
    resid_mid = resid + over_axes(attn_part, TP)
    scaled_mid = (resid_mid * gain_mid.astype(f32)).astype(bf16)
    hidden_part = jnp.dot(scaled_mid, w_ff_in, preferred_element_type=f32)
    square_mid = jnp.sum(resid_mid * resid_mid, axis=1)
    hidden_sum, total_mid = in_one((hidden_part, square_mid), KV)
    inv_mid = lax.rsqrt(total_mid / D + EPS)[:, None]
    hidden = jnp.square(jax.nn.relu(inv_mid * hidden_sum)).astype(bf16)
    out_part = jnp.dot(hidden, w_ff_out, preferred_element_type=f32)
    mixed = (resid_mid + over_axes(out_part, TP)).astype(bf16)
    return (mixed, new_latent, new_rope_key)


def solution(mesh):
    finer = Mesh(mesh.devices.reshape(16, 2, 4, 4), ("kv_0", "kv_1", "tp_0", "tp_1"))
    in_specs = (
        P(None, KV),
        P(),
        P(None, KV_TP, None),
        P(None, KV_TP, None),
        P(KV),
        P(KV, None),
        P(KV, None),
        P(KV, None),
        P(),
        P(),
        P(),
        P(),
        P(),
        P(),
        P(TP, None, KV),
        P(KV),
        P(KV, TP),
        P(TP, KV),
    )
    out_specs = (P(None, KV), P(), P())
    return jax.shard_map(
        per_device, mesh=finer, in_specs=in_specs, out_specs=out_specs, check_vma=False
    )
```

profile of v0, /device:TPU:2, one launch (start us, length us, event | category | flops | bytes accessed | tf_op | source)
XLA Modules:
  0.0 240.8 jit_solution(12234813138934605315)
XLA Ops:
  0.7 0.8 convert_element_type.73
  1.5 0.7 convert_element_type.80
  2.1 0.8 fusion.36
  2.9 0.7 broadcast_compare_fusion
  3.7 0.7 convert_element_type.75
  4.3 0.8 fusion.55
  5.2 0.9 fusion.57
  6.1 1.0 fusion.59
  7.1 62.1 %all-reduce.2 = (f32[16,256]{1,0:T(8,128)S(1)}, f32[16]{0:T(128)S(1)}, f32[16,512]{1,0:T(8,128)S(1)}, f32[16,32]{1,0:T(8,128)S(1)}) all-reduce(f32[16,256]{1,0:T(8,128)S(1)} %fusion.57, f32[16]{0:T(128)S(1)} %fusion.36, f32[16,512]{1,0:T(8,128)S(1)} %fusion.59, ...), channel_id=1, replica_groups=mesh['kv_0'=16,'kv_1'=2,'tp_0'=4,'tp_1'=4] {'kv_0'}, use_global_device_ids=true, to_apply=%region_11.12 | all-reduce | flops 12816 | bytes 102528 | tf_op jit(solution)/shard_map/psum | solution.py:18
  69.2 3.6 %all-reduce.3 = (f32[16,256]{1,0:T(8,128)S(1)}, f32[16]{0:T(128)S(1)}, f32[16,512]{1,0:T(8,128)S(1)}, f32[16,32]{1,0:T(8,128)S(1)}) all-reduce(f32[16,256]{1,0:T(8,128)S(1)} %get-tuple-element.3, f32[16]{0:T(128)S(1)} %get-tuple-element.4, ...), channel_id=1, replica_groups=mesh['kv_0'=16,'kv_1'=2,'tp_0'=4,'tp_1'=4] {'kv_1'}, use_global_device_ids=true, to_apply=%region_12.13 | all-reduce | flops 12816 | bytes 102528 | tf_op jit(solution)/shard_map/psum | solution.py:18
  73.1 1.5 fusion.78
  74.7 0.7 convolution_convert_fusion
  76.2 0.7 copy.58
  76.9 7.5 %all-to-all-start.1 = ((f32[1,16,16]{1,0,2:T(1,128)}), f32[1,16,16]{1,0,2:T(1,128)S(1)}, u32[]{:S(2)}, u32[]{:S(2)}) async-start(f32[1,16,16]{1,0,2:T(1,128)} %copy.58), calls=%async_computation.1 | async-start | bytes 16384 | tf_op jit(solution)/shard_map/all_to_all | solution.py:188
  85.3 0.7 reshape.385
  86.1 0.7 copy.59
  86.8 3.8 %all-to-all-done.1 = f32[1,16,16]{1,0,2:T(1,128)S(1)} async-done(((f32[1,16,16]{1,0,2:T(1,128)}), f32[1,16,16]{1,0,2:T(1,128)S(1)}, u32[]{:S(2)}, u32[]{:S(2)}) %all-to-all-start.1) | async-done | bytes 1056 | tf_op jit(solution)/shard_map/all_to_all | solution.py:188
  90.5 4.7 %all-to-all-start.2 = ((f32[1,16,16]{1,0,2:T(1,128)}), f32[1,16,16]{1,0,2:T(1,128)S(1)}, u32[]{:S(2)}, u32[]{:S(2)}) async-start(f32[1,16,16]{1,0,2:T(1,128)} %copy.59), calls=%async_computation.2 | async-start | bytes 16384 | tf_op jit(solution)/shard_map/all_to_all | solution.py:189
  95.3 6.2 %all-to-all-done.2 = f32[1,16,16]{1,0,2:T(1,128)S(1)} async-done(((f32[1,16,16]{1,0,2:T(1,128)}), f32[1,16,16]{1,0,2:T(1,128)S(1)}, u32[]{:S(2)}, u32[]{:S(2)}) %all-to-all-start.2) | async-done | bytes 1056 | tf_op jit(solution)/shard_map/all_to_all | solution.py:189
  101.5 4.6 %all-to-all-start = ((f32[16,1,1024]{2,1,0:T(1,128)}), f32[16,1,1024]{2,1,0:T(1,128)S(1)}, u32[]{:S(2)}, u32[]{:S(2)}) async-start(f32[16,1,1024]{2,1,0:T(1,128)} %reshape.385), calls=%async_computation | async-start | bytes 131072 | tf_op jit(solution)/shard_map/all_to_all | solution.py:190
  106.1 6.3 %all-to-all-done = f32[16,1,1024]{2,1,0:T(1,128)S(1)} async-done(((f32[16,1,1024]{2,1,0:T(1,128)}), f32[16,1,1024]{2,1,0:T(1,128)S(1)}, u32[]{:S(2)}, u32[]{:S(2)}) %all-to-all-start) | async-done | bytes 65568 | tf_op jit(solution)/shard_map/all_to_all | solution.py:190
  113.0 0.8 reduce.11
  114.0 0.8 reshape.387
  114.9 7.0 %all-to-all-start.3 = ((f32[32,1,1152]{2,1,0:T(1,128)}), f32[32,1,1152]{2,1,0:T(1,128)S(1)}, u32[]{:S(2)}, u32[]{:S(2)}) async-start(f32[32,1,1152]{2,1,0:T(1,128)} %reshape.387), calls=%async_computation.3 | async-start | bytes 294912 | tf_op jit(solution)/shard_map/all_to_all | solution.py:24
  121.9 0.8 fusion.45
  123.1 16.7 %all-to-all-done.3 = f32[32,1,1152]{2,1,0:T(1,128)S(1)} async-done(((f32[32,1,1152]{2,1,0:T(1,128)}), f32[32,1,1152]{2,1,0:T(1,128)S(1)}, u32[]{:S(2)}, u32[]{:S(2)}) %all-to-all-start.3) | async-done | bytes 147488 | tf_op jit(solution)/shard_map/all_to_all | solution.py:24
  139.8 1.0 reduce.12
  142.1 8.9 %psum.92 = f32[16,64]{1,0:T(8,128)S(1)} all-reduce(f32[16,64]{1,0:T(8,128)S(1)} %fusion.5), channel_id=1, replica_groups=mesh['kv_0'=16,'kv_1'=2,'tp_0'=4,'tp_1'=4] {'tp_0'}, use_global_device_ids=true, to_apply=%region_16.17 | all-reduce | flops 1024 | bytes 8192 | tf_op jit(solution)/shard_map/psum | solution.py:18
  151.1 9.3 %psum.93 = f32[16,64]{1,0:T(8,128)S(1)} all-reduce(f32[16,64]{1,0:T(8,128)S(1)} %psum.92), channel_id=1, replica_groups=mesh['kv_0'=16,'kv_1'=2,'tp_0'=4,'tp_1'=4] {'tp_1'}, use_global_device_ids=true, to_apply=%region_17.18 | all-reduce | flops 1024 | bytes 8192 | tf_op jit(solution)/shard_map/psum | solution.py:18
  161.2 60.2 %all_to_all.68 = f32[32,1,8208]{2,1,0:T(1,128)S(1)} all-to-all(f32[32,1,8208]{2,1,0:T(1,128)S(1)} %broadcast_in_dim.38), channel_id=1, replica_groups=mesh['kv_0'=16,'kv_1'=2,'tp_0'=4,'tp_1'=4] {'kv_0','kv_1'}, dimensions={0} | all-to-all | bytes 2101248 | tf_op jit(solution)/shard_map/all_to_all | solution.py:24
  222.4 8.7 %psum.94 = f32[16,64]{1,0:T(8,128)S(1)} all-reduce(f32[16,64]{1,0:T(8,128)S(1)} %fusion.23), channel_id=1, replica_groups=mesh['kv_0'=16,'kv_1'=2,'tp_0'=4,'tp_1'=4] {'tp_0'}, use_global_device_ids=true, to_apply=%region_20.21 | all-reduce | flops 1024 | bytes 8192 | tf_op jit(solution)/shard_map/psum | solution.py:18
  231.2 9.0 %psum.95 = f32[16,64]{1,0:T(8,128)S(1)} all-reduce(f32[16,64]{1,0:T(8,128)S(1)} %psum.94), channel_id=1, replica_groups=mesh['kv_0'=16,'kv_1'=2,'tp_0'=4,'tp_1'=4] {'tp_1'}, use_global_device_ids=true, to_apply=%region_21.22 | all-reduce | flops 1024 | bytes 8192 | tf_op jit(solution)/shard_map/psum | solution.py:18
  (103 shorter events, 7.0 us)
Async XLA Ops:
  0.6 74.0 %copy-start = (bf16[512,16,64]{0,2,1:T(8,128)(2,1)S(1)}, bf16[512,16,64]{0,2,1:T(8,128)(2,1)}, u32[]{:S(2)}) copy-start(bf16[512,16,64]{0,2,1:T(8,128)(2,1)} %param.27) | copy-start | bytes 3145732
  0.6 74.0 %copy-start.3 = (bf16[256,16,64]{0,2,1:T(8,128)(2,1)S(1)}, bf16[256,16,64]{0,2,1:T(8,128)(2,1)}, u32[]{:S(2)}) copy-start(bf16[256,16,64]{0,2,1:T(8,128)(2,1)} %param.30) | copy-start | bytes 1572868
  74.6 0.9 copy-start.5
  74.6 1.2 copy-start.1
  75.8 9.0 %copy-start.2 = (bf16[256,16,64]{0,2,1:T(8,128)(2,1)S(1)}, bf16[256,16,64]{0,2,1:T(8,128)(2,1)}, u32[]{:S(2)}) copy-start(bf16[256,16,64]{0,2,1:T(8,128)(2,1)} %param.31) | copy-start | bytes 1572868
  76.9 13.6 %all-to-all-start.1 = ((f32[1,16,16]{1,0,2:T(1,128)}), f32[1,16,16]{1,0,2:T(1,128)S(1)}, u32[]{:S(2)}, u32[]{:S(2)}) async-start(f32[1,16,16]{1,0,2:T(1,128)} %copy.58), calls=%async_computation.1 | async-start | bytes 16384 | tf_op jit(solution)/shard_map/all_to_all | solution.py:188
  86.1 36.6 %copy-start.10 = (bf16[64]{0:T(256)(128)(2,1)S(1)}, bf16[64]{0:T(256)(128)(2,1)}, u32[]{:S(2)}) copy-start(bf16[64]{0:T(256)(128)(2,1)} %param.33) | copy-start | bytes 388
  86.1 36.6 %copy-start.11 = (bf16[256]{0:T(256)(128)(2,1)S(1)}, bf16[256]{0:T(256)(128)(2,1)}, u32[]{:S(2)}) copy-start(bf16[256]{0:T(256)(128)(2,1)} %param.29) | copy-start | bytes 1540
  90.5 11.0 %all-to-all-start.2 = ((f32[1,16,16]{1,0,2:T(1,128)}), f32[1,16,16]{1,0,2:T(1,128)S(1)}, u32[]{:S(2)}, u32[]{:S(2)}) async-start(f32[1,16,16]{1,0,2:T(1,128)} %copy.59), calls=%async_computation.2 | async-start | bytes 16384 | tf_op jit(solution)/shard_map/all_to_all | solution.py:189
  101.5 11.0 %all-to-all-start = ((f32[16,1,1024]{2,1,0:T(1,128)}), f32[16,1,1024]{2,1,0:T(1,128)S(1)}, u32[]{:S(2)}, u32[]{:S(2)}) async-start(f32[16,1,1024]{2,1,0:T(1,128)} %reshape.385), calls=%async_computation | async-start | bytes 131072 | tf_op jit(solution)/shard_map/all_to_all | solution.py:190
  114.9 24.9 %all-to-all-start.3 = ((f32[32,1,1152]{2,1,0:T(1,128)}), f32[32,1,1152]{2,1,0:T(1,128)S(1)}, u32[]{:S(2)}, u32[]{:S(2)}) async-start(f32[32,1,1152]{2,1,0:T(1,128)} %reshape.387), calls=%async_computation.3 | async-start | bytes 294912 | tf_op jit(solution)/shard_map/all_to_all | solution.py:24
  123.1 18.8 %copy-start.7 = (bf16[16,256]{1,0:T(8,128)(2,1)}, bf16[16,256]{1,0:T(8,128)(2,1)S(1)}, u32[]{:S(2)}) copy-start(bf16[16,256]{1,0:T(8,128)(2,1)S(1)} %get-tuple-element.28) | copy-start | bytes 24580
  140.7 1.1 copy-start.9
  140.9 19.5 %copy-start.4 = (bf16[16,64]{1,0:T(8,128)(2,1)S(1)}, bf16[16,64]{1,0:T(8,128)(2,1)}, u32[]{:S(2)}) copy-start(bf16[16,64]{1,0:T(8,128)(2,1)} %param.18) | copy-start | bytes 6148
  140.9 19.6 %copy-start.6 = (bf16[64,512]{1,0:T(8,128)(2,1)S(1)}, bf16[64,512]{1,0:T(8,128)(2,1)}, u32[]{:S(2)}) copy-start(bf16[64,512]{1,0:T(8,128)(2,1)} %param.34) | copy-start | bytes 196612
  221.4 0.8 copy-start.8
where the time goes:
time: 242 us; the launch traced here: 241 us
  blocking collectives  162 us (67%)
  waiting for transfers between devices  33 us (14%)
  starting transfers between devices  23.7 us (10%)
  other arithmetic  9.57 us (4%)
  matrix products  6.51 us (3%)
  local copies, waits for them, and re-layouts  5 us (2%)
    psum x6, blocking collectives, over_axes(): value = lax.psum(value, axis)  102 us
    all_to_all x1, blocking collectives, copy_for_each(): lax.all_to_all(jnp.broadcast_to(value[None], (size, *value.shape)), axis,...  60.2 us
    all_to_all x1, waiting for transfers between devices, copy_for_each(): lax.all_to_all(jnp.broadcast_to(value[None], (size, *value.shape)), axis,...  16.7 us
    all_to_all x1, starting transfers between devices, per_device(): lax.all_to_all(top[None], TP, split_axis=2, concat_axis=0, tiled=True)  7.48 us
    all_to_all x1, starting transfers between devices, copy_for_each(): lax.all_to_all(jnp.broadcast_to(value[None], (size, *value.shape)), axis,...  6.97 us
    all_to_all x1, waiting for transfers between devices, per_device(): lax.all_to_all(expanded[None], TP, split_axis=2, concat_axis=0, tiled=True)  6.34 us
    all_to_all x1, waiting for transfers between devices, per_device(): lax.all_to_all(total[None], TP, split_axis=2, concat_axis=0, tiled=True)  6.23 us
  transfers between devices with their start and end apart: 4, of which 4 were waited for; matrix products, arithmetic and copies ran while one was open for 1% of the time, Pallas kernels for 0%

commit v1 on v0

--- a/solution.py
+++ b/solution.py
@@ -15,7 +15,7 @@
 
 def over_axes(value, axes):
     for axis in axes:
-        value = lax.psum(value, axis)
+        value = jnp.sum(lax.all_gather(value, axis), axis=0)
     return value
 
 

time: 242 us -> 317 us (1.31)
  blocking collectives: 162 us -> 237 us
  waiting for transfers between devices: 33 us -> 28.1 us
  starting transfers between devices: 23.7 us -> 27.3 us
  local copies, waits for them, and re-layouts: 5 us -> 8.32 us
    all_gather x0 -> x10, blocking collectives: none -> 138 us  [over_axes(): value = jnp.sum(lax.all_gather(value, axis), axis=0)]
    psum x6 -> x0, blocking collectives: 102 us -> none  [over_axes(): value = lax.psum(value, axis)]
    unnamed x0 -> x2, blocking collectives: none -> 38.9 us
    all_to_all x1, waiting for transfers between devices: 3.78 us -> 0.01 us  [per_device(): lax.all_to_all(top[None], TP, split_axis=2, concat_axis=0, tiled=True)]
  transfers between devices with their start and end apart: 4 -> 4, of which waited for: 4 -> 3; matrix products, arithmetic and copies ran while one was open for 1% -> 1% of each run, Pallas kernels for 0% -> 0%
where the time goes in v1:
time: 317 us
  blocking collectives  237 us (75%)
  waiting for transfers between devices  28.1 us (9%)
  starting transfers between devices  27.3 us (9%)
  other arithmetic  9.64 us (3%)
  local copies, waits for them, and re-layouts  8.32 us (3%)
  matrix products  4.03 us (1%)
    all_gather x10, blocking collectives, over_axes(): value = jnp.sum(lax.all_gather(value, axis), axis=0)  138 us
    all_to_all x1, blocking collectives, copy_for_each(): lax.all_to_all(jnp.broadcast_to(value[None], (size, *value.shape)), axis,...  60.2 us
    unnamed x2, blocking collectives  38.9 us
    all_to_all x1, waiting for transfers between devices, copy_for_each(): lax.all_to_all(jnp.broadcast_to(value[None], (size, *value.shape)), axis,...  15.6 us
    all_to_all x1, starting transfers between devices, copy_for_each(): lax.all_to_all(jnp.broadcast_to(value[None], (size, *value.shape)), axis,...  7.93 us
    all_to_all x1, starting transfers between devices, per_device(): lax.all_to_all(top[None], TP, split_axis=2, concat_axis=0, tiled=True)  7.48 us
    all_to_all x1, starting transfers between devices, per_device(): lax.all_to_all(total[None], TP, split_axis=2, concat_axis=0, tiled=True)  7.26 us
  transfers between devices with their start and end apart: 4, of which 3 were waited for; matrix products, arithmetic and copies ran while one was open for 1% of the time, Pallas kernels for 0%

profile of v1, /device:TPU:2, one launch (start us, length us, event | category | flops | bytes accessed | tf_op | source)
XLA Modules:
  0.0 316.8 jit_solution(11516388961491654941)
XLA Ops:
  0.7 1.4 dynamic-slice.5
  2.1 1.3 dynamic-slice.4
  6.0 0.8 fusion.36
  7.0 36.5 %all-reduce.2 = f32[256]{0:T(256)S(1)} all-reduce(f32[256]{0:T(256)S(1)} %dynamic-update-slice), channel_id=2, replica_groups=mesh['kv_0'=16,'kv_1'=2,'tp_0'=4,'tp_1'=4] {'kv_0'}, use_global_device_ids=true, to_apply=%add.2 | all-reduce | flops 256 | bytes 2048
  43.5 0.7 broadcast_compare_fusion
  44.2 0.7 convert_element_type.75
  45.3 2.4 all-reduce.3
  47.8 1.0 fusion.59
  48.9 29.3 %all-gather.2 = f32[256,512]{1,0:T(8,128)S(1)} all-gather(f32[16,512]{1,0:T(8,128)S(1)} %fusion.59), channel_id=4, replica_groups=mesh['kv_0'=16,'kv_1'=2,'tp_0'=4,'tp_1'=4] {'kv_0'}, dimensions={0}, use_global_device_ids=true | all-gather | bytes 557056 | tf_op jit(solution)/shard_map/all_gather | solution.py:18
  78.2 1.9 all-gather.3
  82.5 0.7 copy.58
  83.2 7.5 %all-to-all-start.1 = ((f32[1,16,16]{1,0,2:T(1,128)}), f32[1,16,16]{1,0,2:T(1,128)S(1)}, u32[]{:S(2)}, u32[]{:S(2)}) async-start(f32[1,16,16]{1,0,2:T(1,128)} %copy.58), calls=%async_computation.1 | async-start | bytes 16384 | tf_op jit(solution)/shard_map/all_to_all | solution.py:188
  91.4 28.0 %all-gather.6 = f32[256,32]{1,0:T(8,128)S(1)} all-gather(f32[16,32]{1,0:T(8,128)S(1)} %fusion.55), channel_id=8, replica_groups=mesh['kv_0'=16,'kv_1'=2,'tp_0'=4,'tp_1'=4] {'kv_0'}, dimensions={0}, use_global_device_ids=true | all-gather | bytes 34816 | tf_op jit(solution)/shard_map/all_gather | solution.py:18
  119.5 1.8 all-gather.7
  121.5 28.0 %all-gather.4 = f32[256,256]{1,0:T(8,128)S(1)} all-gather(f32[16,256]{1,0:T(8,128)S(1)} %fusion.57), channel_id=6, replica_groups=mesh['kv_0'=16,'kv_1'=2,'tp_0'=4,'tp_1'=4] {'kv_0'}, dimensions={0}, use_global_device_ids=true | all-gather | bytes 278528 | tf_op jit(solution)/shard_map/all_gather | solution.py:18
  149.7 0.8 fusion.45
  150.5 0.7 reshape.436
  151.9 7.3 %all-to-all-start.2 = ((f32[1,16,16]{1,0,2:T(1,128)}), f32[1,16,16]{1,0,2:T(1,128)S(1)}, u32[]{:S(2)}, u32[]{:S(2)}) async-start(f32[1,16,16]{1,0,2:T(1,128)} %copy.59), calls=%async_computation.2 | async-start | bytes 16384 | tf_op jit(solution)/shard_map/all_to_all | solution.py:189
  159.2 6.2 %all-to-all-done.2 = f32[1,16,16]{1,0,2:T(1,128)S(1)} async-done(((f32[1,16,16]{1,0,2:T(1,128)}), f32[1,16,16]{1,0,2:T(1,128)S(1)}, u32[]{:S(2)}, u32[]{:S(2)}) %all-to-all-start.2) | async-done | bytes 1056 | tf_op jit(solution)/shard_map/all_to_all | solution.py:189
  165.4 4.6 %all-to-all-start = ((f32[16,1,1024]{2,1,0:T(1,128)}), f32[16,1,1024]{2,1,0:T(1,128)S(1)}, u32[]{:S(2)}, u32[]{:S(2)}) async-start(f32[16,1,1024]{2,1,0:T(1,128)} %reshape.436), calls=%async_computation | async-start | bytes 131072 | tf_op jit(solution)/shard_map/all_to_all | solution.py:190
  170.0 6.3 %all-to-all-done = f32[16,1,1024]{2,1,0:T(1,128)S(1)} async-done(((f32[16,1,1024]{2,1,0:T(1,128)}), f32[16,1,1024]{2,1,0:T(1,128)S(1)}, u32[]{:S(2)}, u32[]{:S(2)}) %all-to-all-start) | async-done | bytes 65568 | tf_op jit(solution)/shard_map/all_to_all | solution.py:190
  176.9 0.8 reduce.11
  177.9 0.8 reshape.438
  178.8 7.9 %all-to-all-start.3 = ((f32[32,1,1152]{2,1,0:T(1,128)}), f32[32,1,1152]{2,1,0:T(1,128)S(1)}, u32[]{:S(2)}, u32[]{:S(2)}) async-start(f32[32,1,1152]{2,1,0:T(1,128)} %reshape.438), calls=%async_computation.3 | async-start | bytes 294912 | tf_op jit(solution)/shard_map/all_to_all | solution.py:24
  186.8 1.8 all-gather.5
  189.0 15.6 %all-to-all-done.3 = f32[32,1,1152]{2,1,0:T(1,128)S(1)} async-done(((f32[32,1,1152]{2,1,0:T(1,128)}), f32[32,1,1152]{2,1,0:T(1,128)S(1)}, u32[]{:S(2)}, u32[]{:S(2)}) %all-to-all-start.3) | async-done | bytes 147488 | tf_op jit(solution)/shard_map/all_to_all | solution.py:24
  204.6 1.0 reduce.12
  207.0 11.9 %all-gather.8 = f32[64,64]{1,0:T(8,128)S(1)} all-gather(f32[16,64]{1,0:T(8,128)S(1)} %fusion.5), channel_id=10, replica_groups=mesh['kv_0'=16,'kv_1'=2,'tp_0'=4,'tp_1'=4] {'tp_0'}, dimensions={0}, use_global_device_ids=true | all-gather | bytes 20480 | tf_op jit(solution)/shard_map/all_gather | solution.py:18
  218.9 11.3 %all-gather.9 = f32[64,64]{1,0:T(8,128)S(1)} all-gather(f32[16,64]{1,0:T(8,128)S(1)} %reduce_sum.197), channel_id=11, replica_groups=mesh['kv_0'=16,'kv_1'=2,'tp_0'=4,'tp_1'=4] {'tp_1'}, dimensions={0}, use_global_device_ids=true | all-gather | bytes 20480 | tf_op jit(solution)/shard_map/all_gather | solution.py:18
  231.1 60.2 %all_to_all.68 = f32[32,1,8208]{2,1,0:T(1,128)S(1)} all-to-all(f32[32,1,8208]{2,1,0:T(1,128)S(1)} %broadcast_in_dim.35), channel_id=1, replica_groups=mesh['kv_0'=16,'kv_1'=2,'tp_0'=4,'tp_1'=4] {'kv_0','kv_1'}, dimensions={0} | all-to-all | bytes 2101248 | tf_op jit(solution)/shard_map/all_to_all | solution.py:24
  292.3 11.9 %all-gather.10 = f32[64,64]{1,0:T(8,128)S(1)} all-gather(f32[16,64]{1,0:T(8,128)S(1)} %fusion.23), channel_id=12, replica_groups=mesh['kv_0'=16,'kv_1'=2,'tp_0'=4,'tp_1'=4] {'tp_0'}, dimensions={0}, use_global_device_ids=true | all-gather | bytes 20480 | tf_op jit(solution)/shard_map/all_gather | solution.py:18
  304.2 11.9 %all-gather.11 = f32[64,64]{1,0:T(8,128)S(1)} all-gather(f32[16,64]{1,0:T(8,128)S(1)} %reduce_sum.201), channel_id=13, replica_groups=mesh['kv_0'=16,'kv_1'=2,'tp_0'=4,'tp_1'=4] {'tp_1'}, dimensions={0}, use_global_device_ids=true | all-gather | bytes 20480 | tf_op jit(solution)/shard_map/all_gather | solution.py:18
  (135 shorter events, 11.2 us)
Async XLA Ops:
  0.6 80.2 %copy-start = (bf16[512,16,64]{0,2,1:T(8,128)(2,1)S(1)}, bf16[512,16,64]{0,2,1:T(8,128)(2,1)}, u32[]{:S(2)}) copy-start(bf16[512,16,64]{0,2,1:T(8,128)(2,1)} %param.27) | copy-start | bytes 3145732
  0.6 79.7 %copy-start.3 = (bf16[512,16,32]{0,2,1:T(8,128)(2,1)S(1)}, bf16[512,16,32]{0,2,1:T(8,128)(2,1)}, u32[]{:S(2)}) copy-start(bf16[512,16,32]{0,2,1:T(8,128)(2,1)} %param.28) | copy-start | bytes 1572868
  47.8 33.0 %copy-start.4 = (bf16[256,16,64]{0,2,1:T(8,128)(2,1)S(1)}, bf16[256,16,64]{0,2,1:T(8,128)(2,1)}, u32[]{:S(2)}) copy-start(bf16[256,16,64]{0,2,1:T(8,128)(2,1)} %param.30) | copy-start | bytes 1572868
  80.9 0.9 copy-start.6
  80.9 1.2 copy-start.1
  82.1 9.0 %copy-start.5 = (bf16[16,64]{1,0:T(8,128)(2,1)S(1)}, bf16[16,64]{1,0:T(8,128)(2,1)}, u32[]{:S(2)}) copy-start(bf16[16,64]{1,0:T(8,128)(2,1)} %param.18) | copy-start | bytes 6148
  82.1 9.0 %copy-start.9 = (bf16[64,32]{0,1:T(8,128)(2,1)S(1)}, bf16[64,32]{0,1:T(8,128)(2,1)}, u32[]{:S(2)}) copy-start(bf16[64,32]{0,1:T(8,128)(2,1)} %param.25) | copy-start | bytes 12292
  82.1 9.2 %copy-start.8 = (bf16[64,256]{1,0:T(8,128)(2,1)S(1)}, bf16[64,256]{1,0:T(8,128)(2,1)}, u32[]{:S(2)}) copy-start(bf16[64,256]{1,0:T(8,128)(2,1)} %param.24) | copy-start | bytes 98308
  82.5 67.0 %copy-start.2 = (bf16[256,16,64]{0,2,1:T(8,128)(2,1)S(1)}, bf16[256,16,64]{0,2,1:T(8,128)(2,1)}, u32[]{:S(2)}) copy-start(bf16[256,16,64]{0,2,1:T(8,128)(2,1)} %param.31) | copy-start | bytes 1572868
  83.2 68.7 %all-to-all-start.1 = ((f32[1,16,16]{1,0,2:T(1,128)}), f32[1,16,16]{1,0,2:T(1,128)S(1)}, u32[]{:S(2)}, u32[]{:S(2)}) async-start(f32[1,16,16]{1,0,2:T(1,128)} %copy.58), calls=%async_computation.1 | async-start | bytes 16384 | tf_op jit(solution)/shard_map/all_to_all | solution.py:188
  150.5 36.2 %copy-start.13 = (bf16[64]{0:T(256)(128)(2,1)S(1)}, bf16[64]{0:T(256)(128)(2,1)}, u32[]{:S(2)}) copy-start(bf16[64]{0:T(256)(128)(2,1)} %param.33) | copy-start | bytes 388
  150.5 36.2 %copy-start.14 = (bf16[256]{0:T(256)(128)(2,1)S(1)}, bf16[256]{0:T(256)(128)(2,1)}, u32[]{:S(2)}) copy-start(bf16[256]{0:T(256)(128)(2,1)} %param.29) | copy-start | bytes 1540
  151.9 13.5 %all-to-all-start.2 = ((f32[1,16,16]{1,0,2:T(1,128)}), f32[1,16,16]{1,0,2:T(1,128)S(1)}, u32[]{:S(2)}, u32[]{:S(2)}) async-start(f32[1,16,16]{1,0,2:T(1,128)} %copy.59), calls=%async_computation.2 | async-start | bytes 16384 | tf_op jit(solution)/shard_map/all_to_all | solution.py:189
  165.4 11.0 %all-to-all-start = ((f32[16,1,1024]{2,1,0:T(1,128)}), f32[16,1,1024]{2,1,0:T(1,128)S(1)}, u32[]{:S(2)}, u32[]{:S(2)}) async-start(f32[16,1,1024]{2,1,0:T(1,128)} %reshape.436), calls=%async_computation | async-start | bytes 131072 | tf_op jit(solution)/shard_map/all_to_all | solution.py:190
  178.8 25.8 %all-to-all-start.3 = ((f32[32,1,1152]{2,1,0:T(1,128)}), f32[32,1,1152]{2,1,0:T(1,128)S(1)}, u32[]{:S(2)}, u32[]{:S(2)}) async-start(f32[32,1,1152]{2,1,0:T(1,128)} %reshape.438), calls=%async_computation.3 | async-start | bytes 294912 | tf_op jit(solution)/shard_map/all_to_all | solution.py:24
  189.0 17.7 %copy-start.10 = (bf16[16,256]{1,0:T(8,128)(2,1)}, bf16[16,256]{1,0:T(8,128)(2,1)S(1)}, u32[]{:S(2)}) copy-start(bf16[16,256]{1,0:T(8,128)(2,1)S(1)} %get-tuple-element.20) | copy-start | bytes 24580
  205.6 1.1 copy-start.12
  205.8 24.6 %copy-start.7 = (bf16[64,512]{1,0:T(8,128)(2,1)S(1)}, bf16[64,512]{1,0:T(8,128)(2,1)}, u32[]{:S(2)}) copy-start(bf16[64,512]{1,0:T(8,128)(2,1)} %param.34) | copy-start | bytes 196612
  291.3 0.8 copy-start.11
